TPU v7x, 32 devices: a whole 2x2x4 slice. The times are simulated.
32 devices in a mesh: sp: 8 (over z, x), tp: 4 (over y, core).
Axes of the slice: x: 2, y: 2, z: 4, core: 2. Of those that a mesh axis runs over, the one named last changes fastest.
Arguments:
- residual_in: bfloat16 [2048, 2048], P('sp', 'tp'), may hold values from -6 to 6
- conv_input: bfloat16 [2048, 512], P('sp', 'tp'), may hold values from -6 to 6
- outer_gate: bfloat16 [2048, 512], P('sp', 'tp'), may hold values from -6 to 6
- inner_gate: bfloat16 [2048, 512], P('sp', 'tp'), may hold values from -6 to 6
- documents: int32 [2048], P('sp'), may hold values from 0 to 3, as said below
- conv_taps: float32 [3, 512], P(None, 'tp'), may hold values from -3 to 3
- mixer_gain: float32 [512], replicated, may hold values from 0.1 to 1.9
- output_weight: bfloat16 [512, 2048], P(None, 'tp'), may hold values from -0.25 to 0.25
- ffn_gain: float32 [2048], P('tp'), may hold values from 0.1 to 1.9
- routes: int32 [2048, 2], P('sp'), may hold values from 0 to 7, all different within a row; in each aligned block of 256 rows (0 to 255, 256 to 511, ...) at most 128 rows name the same one
- route_weights: float32 [2048, 2], P('sp'), may hold values from 0.1 to 0.9
- expert_gate: bfloat16 [8, 2048, 3584], P('sp', None, 'tp'), may hold values from -0.125 to 0.125
- expert_up: bfloat16 [8, 2048, 3584], P('sp', None, 'tp'), may hold values from -0.125 to 0.125
- expert_down: bfloat16 [8, 3584, 2048], P('sp', 'tp'), may hold values from -0.09375 to 0.09375
Outputs:
- layer_out: bfloat16 [2048, 2048], P('sp', 'tp')
Inputs may be any that keep to these rules, and one draw needn't show every extreme that they name: Document numbers never fall along the positions, and each of the 4 documents occurs. Every document has 256 to 768 positions, and one has exactly 768. `routes`: the two experts of a position differ. Among the 256 positions of one index of sp no expert is named more than 128 times, a bound that some block reaches.
All inputs are finite; a program needn't handle non-finite values.
Results may differ from a plain program's by a relative error of at most 0.0058.
Values may be sent and summed in bfloat16 or wider, within the bound.
A program may use at most 64 MiB of HBM per device.

v0:
```python
import functools

import jax
import jax.numpy as jnp
from jax import lax
from jax.experimental import pallas as pl
from jax.experimental.pallas import tpu as pltpu
from jax.sharding import PartitionSpec as P

EPS = 1e-06
MESH = pl.DeviceIdType.MESH


def layer_kernel(
    n,
    group,
    residual_hbm,
    conv_input,
    outer_gate,
    inner_gate,
    documents,
    conv_taps,
    mixer_gain,
    ow_hbm,
    ffn_gain,
    routes,
    route_weights,
    gate_hbm,
    up_hbm,
    down_hbm,
    layer_out,
    residual,
    ow,
    halo_conv,
    halo_inner,
    halo_docs,
    joined,
    joined_docs,
    mixbuf,
    totals,
    hidden,
    normed,
    outgoing,
    returned,
    wg,
    wu,
    wd,
    arrived,
    act,
    msend,
    mrecv,
    mine,
    ysend,
    yrecv,
    mine2,
    rsend,
    w_sem,
    a2a_s,
    a2a_r,
    agy_s,
    agy_r,
    agm_s,
    agm_r,
    agf_s,
    agf_r,
    rsm_s,
    rsm_r,
    rsy_s,
    rsy_r,
    ret_s,
    ret_r,
    halo_s,
    halo_r,
    mix_s,
    mix_r,
    tot_s,
    tot_r,
):
    me = lax.axis_index("sp")
    t = lax.axis_index("tp")
    a = t // 2
    b = t % 2
    mate = 2 * a + (1 - b)
    partner = 2 * (1 - a) + b
    across = 2 * (1 - a) + (1 - b)
    cap, lf = outgoing.shape[1], outgoing.shape[2]
    units = wg.shape[1]
    tokens = conv_input.shape[0]
    chans = conv_input.shape[1]
    rows = group * cap
    steps = n // group

    early = [
        pltpu.make_async_copy(ow_hbm, ow, w_sem.at[3]),
        pltpu.make_async_copy(residual_hbm, residual, w_sem.at[4]),
    ]
    loads = [
        pltpu.make_async_copy(gate_hbm.at[0], wg, w_sem.at[0]),
        pltpu.make_async_copy(up_hbm.at[0], wu, w_sem.at[1]),
        pltpu.make_async_copy(down_hbm.at[0], wd, w_sem.at[2]),
    ]
    for load in early + loads:
        load.start()

    barrier = pltpu.get_barrier_semaphore()

    def greet(p, c):
        pl.semaphore_signal(
            barrier, inc=1, device_id={"sp": (me + p) % n}, device_id_type=MESH
        )
        return c

    lax.fori_loop(1, n, greet, 0)
    for other in (mate, partner, across):
        pl.semaphore_signal(barrier, inc=1, device_id={"tp": other}, device_id_type=MESH)
    pl.semaphore_wait(barrier, n + 2)

    def remote(src, dst, s, r, dev):
        return pltpu.make_async_remote_copy(
            src_ref=src, dst_ref=dst, send_sem=s, recv_sem=r, device_id=dev, device_id_type=MESH
        )

    def span(p):
        return pl.ds(pl.multiple_of(p * cap, cap), cap)

    def span_g(i):
        return pl.ds(pl.multiple_of(i * rows, rows), rows)

    def a2a(p):
        return remote(
            outgoing.at[(me + p) % n],
            arrived.at[t, span(p)],
            a2a_s.at[p],
            a2a_r.at[p],
            {"sp": (me + p) % n},
        )

    def slab(p):
        return arrived.at[t, span(p)]

    def agy(p):
        return remote(slab(p), slab(p), agy_s.at[p], agy_r.at[p], {"tp": partner})

    def agm(p):
        return remote(slab(p), slab(p), agm_s.at[p], agm_r.at[p], {"tp": mate})

    def agf(p):
        piece = arrived.at[partner, span(p)]
        return remote(piece, piece, agf_s.at[p], agf_r.at[p], {"tp": mate})

    def rsm(i, h):
        return remote(
            msend.at[i, h], mrecv.at[i, h], rsm_s.at[i, h], rsm_r.at[i, h], {"tp": mate}
        )

    def rsy(p):
        return remote(
            ysend.at[span(p)], yrecv.at[span(p)], rsy_s.at[p], rsy_r.at[p], {"tp": partner}
        )

    def ret(p):
        return remote(
            rsend.at[span(p)],
            returned.at[span(p)],
            ret_s.at[p],
            ret_r.at[p],
            {"sp": (me + n - p) % n},
        )

    def each(low, high, f):
        def one(p, c):
            f(p)
            return c

        lax.fori_loop(low, high, one, 0)

    others = (mate, partner, across)

    @pl.when(me == 0)
    def _():
        halo_conv[...] = jnp.zeros_like(halo_conv)
        halo_inner[...] = jnp.zeros_like(halo_inner)
        halo_docs[...] = jnp.full_like(halo_docs, -1)

    def halo(j):
        last = pl.ds(tokens - 16, 16)
        src = (conv_input.at[last], inner_gate.at[last], documents)[j]
        dst = (halo_conv, halo_inner, halo_docs)[j]
        return remote(src, dst, halo_s.at[j], halo_r.at[j], {"sp": (me + 1) % n})

    @pl.when(me < n - 1)
    def _():
        for j in range(3):
            halo(j).start()

    f32, bf = jnp.float32, jnp.bfloat16
    row_id = lax.broadcasted_iota(jnp.int32, (tokens, tokens), 0)
    col_id = lax.broadcasted_iota(jnp.int32, (tokens, tokens), 1)
    eye = row_id == col_id

    def to_column(row):
        return jnp.sum(jnp.where(eye, row, 0.0), axis=1, keepdims=True)

    def to_row(column):
        return jnp.sum(jnp.where(eye, column, 0.0), axis=0, keepdims=True)

    expert_id = lax.broadcasted_iota(jnp.int32, (n, tokens), 0)
    hot = [(expert_id == routes[k : k + 1, :]).astype(f32) for k in range(2)]
    before = (row_id < col_id).astype(bf)
    counts = jnp.dot((hot[0] + hot[1]).astype(bf), before, preferred_element_type=f32)
    slots = [
        jnp.sum(hot[k] * (counts + (expert_id * cap).astype(f32)), axis=0, keepdims=True)
        for k in range(2)
    ]
    slot_rows = [s.astype(jnp.int32) for s in slots]
    slot_cols = []
    for s in slots:
        near = s.astype(jnp.int32) - me * cap
        near = jnp.where(near < 0, near + n * cap, near)
        slot_cols.append(to_column(near.astype(f32)).astype(jnp.int32))

    own = (inner_gate[...].astype(f32) * conv_input[...].astype(f32)).astype(bf).astype(f32)
    joined[pl.ds(16, tokens), :] = own
    doc_col = to_column(documents[...].astype(f32))
    joined_docs[pl.ds(16, tokens), :] = jnp.broadcast_to(doc_col, (tokens, chans))

    @pl.when(me > 0)
    def _():
        for j in range(3):
            halo(j).wait_recv()

    joined[pl.ds(0, 16), :] = (
        (halo_inner[...].astype(f32) * halo_conv[...].astype(f32)).astype(bf).astype(f32)
    )
    halo_col = to_column(halo_docs[...].astype(f32))
    joined_docs[pl.ds(0, 16), :] = jnp.broadcast_to(halo_col[tokens - 16 :, :], (16, chans))
    docs_here = joined_docs[pl.ds(16, tokens), :]
    same_one = (joined_docs[pl.ds(15, tokens), :] == docs_here).astype(f32)
    same_two = (joined_docs[pl.ds(14, tokens), :] == docs_here).astype(f32)
    conv_sum = (
        conv_taps[2:3, :] * own
        + conv_taps[1:2, :] * joined[pl.ds(15, tokens), :] * same_one
        + conv_taps[0:1, :] * joined[pl.ds(14, tokens), :] * same_two
    )
    mixbuf[t] = (outer_gate[...].astype(f32) * conv_sum).astype(bf)

    def mix(j):
        return remote(
            mixbuf.at[t], mixbuf.at[t], mix_s.at[j], mix_r.at[j], {"tp": others[j]}
        )

    for j in (1, 2, 0):
        mix(j).start()
    for load in early:
        load.wait()
    for j in range(3):
        mix(j).wait_recv()
    accum = None
    squares = None
    for q in range(4):
        piece = mixbuf[q].astype(f32)
        deep = slice(q * chans, (q + 1) * chans)
        scaled = (piece * mixer_gain[0:1, deep]).astype(bf)
        part = jnp.dot(scaled, ow[deep, :], preferred_element_type=f32)
        square = jnp.sum(piece * piece, axis=1, keepdims=True)
        accum = part if accum is None else accum + part
        squares = square if squares is None else squares + square
    mix_scale = lax.rsqrt(squares / (4 * chans) + EPS)
    hidden[...] = residual[...].astype(f32) + accum * mix_scale
    state = hidden[...]
    total = to_row(jnp.sum(state * state, axis=1, keepdims=True))
    totals[t] = jnp.broadcast_to(total, (8, tokens))

    def tot(j):
        return remote(
            totals.at[t], totals.at[t], tot_s.at[j], tot_r.at[j], {"tp": others[j]}
        )

    for j in (1, 2, 0):
        tot(j).start()
    for j in range(3):
        tot(j).wait_recv()
    feature_total = to_column((totals[0] + totals[1] + totals[2] + totals[3])[0:1, :])
    normed[...] = (
        hidden[...] * lax.rsqrt(feature_total / (4 * lf) + EPS) * ffn_gain[...]
    ).astype(bf)

    def pick_for(e):
        slot_id = lax.broadcasted_iota(jnp.int32, (cap, tokens), 0) + e * cap
        pick = (slot_id == slot_rows[0]) | (slot_id == slot_rows[1])
        return jnp.dot(
            pick.astype(f32).astype(bf), normed[...], preferred_element_type=f32
        ).astype(bf)

    def dispatch(p):
        e = (me + p) % n
        outgoing[e] = pick_for(e)
        a2a(p).start()

    arrived[t, pl.ds(0, cap), :] = pick_for(me)
    agy(0).start()
    agm(0).start()
    each(1, n, dispatch)

    def spread(p):
        a2a(p).wait_recv()
        agy(p).start()
        agm(p).start()

    def relay(p):
        agy(p).wait_recv()
        agf(p).start()

    def settle(p):
        agm(p).wait_recv()
        agf(p).wait_recv()

    def over_group(i, f):
        each(i * group, (i + 1) * group, f)

    def reduce_mate(i):
        rsm(i, 0).wait_recv()
        ysend[span_g(i), :] = (mine[0] + mrecv[i, 0].astype(jnp.float32)).astype(jnp.bfloat16)
        over_group(i, lambda p: rsy(p).start())
        rsm(i, 1).wait_recv()
        mine2[...] = mine[1] + mrecv[i, 1].astype(jnp.float32)

    def reduce_partner(i):
        def back(p):
            rsy(p).wait_recv()
            local = pl.ds(pl.multiple_of((p - i * group) * cap, cap), cap)
            rsend[span(p), :] = (
                mine2[local, :] + yrecv[span(p), :].astype(jnp.float32)
            ).astype(jnp.bfloat16)

            @pl.when(p > 0)
            def _():
                ret(p).start()

        over_group(i, back)

    def compute(i):
        whole = jnp.concatenate([arrived[q, span_g(i), :] for q in range(4)], axis=1)
        for j in range(units // 128):
            cols = slice(j * 128, (j + 1) * 128)
            w = jnp.concatenate([wg[:, cols], wu[:, cols]], axis=1)
            both = jnp.dot(whole, w, preferred_element_type=jnp.float32)
            g = both[:, :128]
            act[:, cols] = (g * jax.nn.sigmoid(g) * both[:, 128:]).astype(jnp.bfloat16)
        for h in range(2):
            qa = (1 - a) if h == 0 else a
            far = pl.ds(pl.multiple_of((2 * qa + 1 - b) * lf, lf), lf)
            near = pl.ds(pl.multiple_of((2 * qa + b) * lf, lf), lf)
            msend[i, h] = jnp.dot(
                act[...], wd[:, far], preferred_element_type=jnp.float32
            ).astype(jnp.bfloat16)
            rsm(i, h).start()
            mine[h] = jnp.dot(act[...], wd[:, near], preferred_element_type=jnp.float32)

    each(1, group, spread)
    if steps > 1:
        over_group(1, spread)
    for load in loads:
        load.wait()

    def step(i, c):
        over_group(i, relay)

        @pl.when(i > 0)
        def _():
            reduce_mate(i - 1)

        over_group(i, settle)

        @pl.when(i + 2 < steps)
        def _():
            over_group(i + 2, spread)

        compute(i)

        @pl.when(i > 0)
        def _():
            reduce_partner(i - 1)

        return c

    lax.fori_loop(0, steps, step, 0)
    reduce_mate(steps - 1)

    weight_cols = [to_column(route_weights[k : k + 1, :]) for k in range(2)]

    def combine(i):
        def came(p):
            @pl.when(p > 0)
            def _():
                ret(p).wait_recv()

        over_group(i, came)
        if i == 0:
            here = jnp.concatenate(
                [rsend[0:cap, :], returned[cap:rows, :]], axis=0
            ) if group > 1 else rsend[0:cap, :]
        else:
            here = returned[i * rows : (i + 1) * rows, :]
        slot_id = lax.broadcasted_iota(jnp.int32, (tokens, rows), 1) + i * rows
        total = hidden[...]
        for k in range(2):
            pick = (slot_id == slot_cols[k]).astype(f32).astype(bf)
            picked = jnp.dot(pick, here, preferred_element_type=f32)
            total = total + picked * weight_cols[k]
        return total

    for i in range(steps - 2):
        hidden[...] = combine(i)
    reduce_partner(steps - 1)
    for i in range(max(0, steps - 2), steps - 1):
        hidden[...] = combine(i)
    layer_out[...] = combine(steps - 1).astype(bf)


    def finish(p):
        agy(p).wait_send()
        agm(p).wait_send()
        agf(p).wait_send()

        @pl.when(p > 0)
        def _():
            a2a(p).wait_send()
            ret(p).wait_send()

    each(0, n, finish)

    each(0, n, lambda p: rsy(p).wait_send())

    def finish_group(i):
        rsm(i, 0).wait_send()
        rsm(i, 1).wait_send()

    each(0, steps, finish_group)
    for j in range(3):
        mix(j).wait_send()
        tot(j).wait_send()

    @pl.when(me < n - 1)
    def _():
        for j in range(3):
            halo(j).wait_send()


def per_device(
    residual_in,
    conv_input,
    outer_gate,
    inner_gate,
    documents,
    conv_taps,
    mixer_gain,
    output_weight,
    ffn_gain,
    routes,
    route_weights,
    expert_gate,
    expert_up,
    expert_down,
):
    tokens, lf = residual_in.shape
    chans = conv_input.shape[1]
    n = lax.axis_size("sp") * expert_gate.shape[0]
    cap = 4 * tokens // n
    width, units = expert_gate.shape[1:]
    group = max(1, min(n, 256 // cap))
    rows, steps = group * cap, n // group
    bf, f32 = jnp.bfloat16, jnp.float32
    dma = pltpu.SemaphoreType.DMA
    vmem, hbm = pl.BlockSpec(memory_space=pltpu.VMEM), pl.BlockSpec(memory_space=pl.ANY)
    return pl.pallas_call(
        functools.partial(layer_kernel, n, group),
        out_shape=jax.ShapeDtypeStruct((tokens, lf), bf),
        in_specs=[hbm] + [vmem] * 6 + [hbm] + [vmem] * 3 + [hbm] * 3,
        out_specs=vmem,
        scratch_shapes=[
            pltpu.VMEM((tokens, lf), bf),
            pltpu.VMEM(output_weight.shape, bf),
            pltpu.VMEM((16, chans), bf),
            pltpu.VMEM((16, chans), bf),
            pltpu.VMEM((1, tokens), jnp.int32),
            pltpu.VMEM((tokens + 16, chans), f32),
            pltpu.VMEM((tokens + 16, chans), f32),
            pltpu.VMEM((4, tokens, chans), bf),
            pltpu.VMEM((4, 8, tokens), f32),
            pltpu.VMEM((tokens, lf), f32),
            pltpu.VMEM((tokens, lf), bf),
            pltpu.VMEM((n, cap, lf), bf),
            pltpu.VMEM((n * cap, lf), bf),
            pltpu.VMEM((width, units), bf),
            pltpu.VMEM((width, units), bf),
            pltpu.VMEM((units, width), bf),
            pltpu.VMEM((4, n * cap, lf), bf),
            pltpu.VMEM((rows, units), bf),
            pltpu.VMEM((steps, 2, rows, lf), bf),
            pltpu.VMEM((steps, 2, rows, lf), bf),
            pltpu.VMEM((2, rows, lf), f32),
            pltpu.VMEM((n * cap, lf), bf),
            pltpu.VMEM((n * cap, lf), bf),
            pltpu.VMEM((rows, lf), f32),
            pltpu.VMEM((n * cap, lf), bf),
            dma((5,)),
        ]
        + [dma((n,))] * 8
        + [dma((steps, 2))] * 2
        + [dma((n,))] * 4
        + [dma((3,))] * 6,
        compiler_params=pltpu.CompilerParams(
            collective_id=0, has_side_effects=True, vmem_limit_bytes=58 * 1024 * 1024
        ),
        name="layer",
    )(
        residual_in,
        conv_input,
        outer_gate,
        inner_gate,
        documents.reshape(1, tokens),
        conv_taps,
        mixer_gain.reshape(1, -1),
        output_weight,
        ffn_gain.reshape(1, -1),
        routes.T,
        route_weights.T,
        expert_gate,
        expert_up,
        expert_down,
    )


def solution(mesh):
    placed = (
        P("sp", "tp"),
        P("sp", "tp"),
        P("sp", "tp"),
        P("sp", "tp"),
        P("sp"),
        P(None, "tp"),
        P(),
        P(None, "tp"),
        P("tp"),
        P("sp", None),
        P("sp", None),
        P("sp", None, "tp"),
        P("sp", None, "tp"),
        P("sp", "tp", None),
    )
    return jax.shard_map(
        per_device, mesh=mesh, in_specs=placed, out_specs=P("sp", "tp"), check_vma=False
    )
```

profile of v0, /device:TPU:0, one launch (start us, length us, event | category | flops | bytes accessed | tf_op | source)
XLA Modules:
  0.0 93.3 jit_solution(2461211645740285553)
XLA Ops:
  0.0 91.6 %layer.1 = bf16[256,512]{1,0:T(8,128)(2,1)} custom-call(bf16[256,512]{1,0:T(8,128)(2,1)} %residual_hbm.1, bf16[256,128]{1,0:T(8,128)(2,1)} %conv_input.1, bf16[256,128]{1,0:T(8,128)(2,1)} %outer_gate.1, bf16[256,128]{1,0:T(8,128)(2,1)} %inner_gate.1, s32[1,256]{1,0:T(1,128)} %bitcast.9, f32[3,128]{1,0:T(4,128)} %conv_taps.1, f32[1,512]{1,0:T(1,128)} %bitcast.5, ...), custom_call_target="tpu_custom_call" | custom-call | tf_op jit(solution)/shard_map/layer/pallas_call | solution.py:476
  91.6 1.7 %copy.16 = bf16[256,512]{1,0:T(8,128)(2,1)} copy(bf16[256,512]{1,0:T(8,128)(2,1)} %layer.1) | data formatting | bytes 524288
where the time goes:
time: 93.5 us; the launch traced here: 93.3 us
  Pallas kernels  91.6 us (98%)
  local copies, waits for them, and re-layouts  1.67 us (2%)
    pallas_call x1, Pallas kernels, per_device(): pl.pallas_call(functools.partial(layer_kernel, n, group), out_shape=jax.S...  91.6 us

commit v1 on v0

--- a/solution.py
+++ b/solution.py
@@ -9,6 +9,14 @@
 
 EPS = 1e-06
 MESH = pl.DeviceIdType.MESH
+
+
+ISSUE = "Z123"
+PLAN = (
+    "00", "S1", "W0", "X0", "Y0", "T0", "C0", "S2", "S3", "Y1", "T1", "C1",
+    "Y2", "T2", "C2", "M2", "Y3", "T3", "C3", "M3", "M1", "M0", "P2", "P3",
+    "G0", "P1", "P0", "K0", "F0",
+)
 
 
 def layer_kernel(
@@ -52,7 +60,6 @@
     mine,
     ysend,
     yrecv,
-    mine2,
     rsend,
     w_sem,
     a2a_s,
@@ -75,6 +82,13 @@
     mix_r,
     tot_s,
     tot_r,
+    far_s,
+    far_r,
+    far_routes,
+    far_weights,
+    far_normed,
+    far_send,
+    far_sum,
 ):
     me = lax.axis_index("sp")
     t = lax.axis_index("tp")
@@ -104,16 +118,13 @@
 
     barrier = pltpu.get_barrier_semaphore()
 
-    def greet(p, c):
-        pl.semaphore_signal(
-            barrier, inc=1, device_id={"sp": (me + p) % n}, device_id_type=MESH
-        )
+    def greet(q, c):
+        pl.semaphore_signal(barrier, inc=1, device_id={"sp": me ^ q}, device_id_type=MESH)
         return c
 
     lax.fori_loop(1, n, greet, 0)
     for other in (mate, partner, across):
         pl.semaphore_signal(barrier, inc=1, device_id={"tp": other}, device_id_type=MESH)
-    pl.semaphore_wait(barrier, n + 2)
 
     def remote(src, dst, s, r, dev):
         return pltpu.make_async_remote_copy(
@@ -128,11 +139,11 @@
 
     def a2a(p):
         return remote(
-            outgoing.at[(me + p) % n],
+            outgoing.at[me ^ p],
             arrived.at[t, span(p)],
             a2a_s.at[p],
             a2a_r.at[p],
-            {"sp": (me + p) % n},
+            {"sp": me ^ (p % (n // 2))},
         )
 
     def slab(p):
@@ -164,7 +175,7 @@
             returned.at[span(p)],
             ret_s.at[p],
             ret_r.at[p],
-            {"sp": (me + n - p) % n},
+            {"sp": me ^ (p % (n // 2))},
         )
 
     def each(low, high, f):
@@ -174,13 +185,65 @@
 
         lax.fori_loop(low, high, one, 0)
 
+    def over_group(i, f):
+        each(i * group, (i + 1) * group, f)
+
     others = (mate, partner, across)
 
-    @pl.when(me == 0)
-    def _():
-        halo_conv[...] = jnp.zeros_like(halo_conv)
-        halo_inner[...] = jnp.zeros_like(halo_inner)
-        halo_docs[...] = jnp.full_like(halo_docs, -1)
+    f32, bf = jnp.float32, jnp.bfloat16
+    row_id = lax.broadcasted_iota(jnp.int32, (tokens, tokens), 0)
+    col_id = lax.broadcasted_iota(jnp.int32, (tokens, tokens), 1)
+    eye = row_id == col_id
+
+    def to_column(row):
+        return jnp.sum(jnp.where(eye, row, 0.0), axis=1, keepdims=True)
+
+    def to_row(column):
+        return jnp.sum(jnp.where(eye, column, 0.0), axis=0, keepdims=True)
+
+    expert_id = lax.broadcasted_iota(jnp.int32, (n, tokens), 0)
+    before = (row_id < col_id).astype(bf)
+    away = n // 2
+    twin = me ^ away
+
+    def ranks(table):
+        hot = [(expert_id == table[k : k + 1, :]).astype(f32) for k in range(2)]
+        return hot, jnp.dot((hot[0] + hot[1]).astype(bf), before, preferred_element_type=f32)
+
+    def places(ranked, block):
+        hot, counts = ranked
+        return [
+            jnp.sum(hot[k] * (counts + (block * cap).astype(f32)), axis=0, keepdims=True)
+            for k in range(2)
+        ]
+
+    def as_columns(found):
+        return [to_column(v).astype(jnp.int32) for v in found]
+
+    own_ranks = ranks(routes)
+    slot_rows = [v.astype(jnp.int32) for v in places(own_ranks, expert_id)]
+    slot_cols = as_columns(places(own_ranks, expert_id ^ me))
+    weight_cols = [to_column(route_weights[k : k + 1, :]) for k in range(2)]
+
+    own = (inner_gate[...].astype(f32) * conv_input[...].astype(f32)).astype(bf).astype(f32)
+    joined[pl.ds(16, tokens), :] = own
+    doc_col = to_column(documents[...].astype(f32))
+    joined_docs[pl.ds(16, tokens), :] = jnp.broadcast_to(doc_col, (tokens, chans))
+
+    def convolve(first, count):
+        here = joined_docs[pl.ds(first + 16, count), :]
+        same_one = (joined_docs[pl.ds(first + 15, count), :] == here).astype(f32)
+        same_two = (joined_docs[pl.ds(first + 14, count), :] == here).astype(f32)
+        conv_sum = (
+            conv_taps[2:3, :] * joined[pl.ds(first + 16, count), :]
+            + conv_taps[1:2, :] * joined[pl.ds(first + 15, count), :] * same_one
+            + conv_taps[0:1, :] * joined[pl.ds(first + 14, count), :] * same_two
+        )
+        gate = outer_gate[pl.ds(first, count), :].astype(f32)
+        mixbuf[t, pl.ds(first, count), :] = (gate * conv_sum).astype(bf)
+
+    convolve(16, tokens - 16)
+    pl.semaphore_wait(barrier, n + 2)
 
     def halo(j):
         last = pl.ds(tokens - 16, 16)
@@ -193,67 +256,51 @@
         for j in range(3):
             halo(j).start()
 
-    f32, bf = jnp.float32, jnp.bfloat16
-    row_id = lax.broadcasted_iota(jnp.int32, (tokens, tokens), 0)
-    col_id = lax.broadcasted_iota(jnp.int32, (tokens, tokens), 1)
-    eye = row_id == col_id
-
-    def to_column(row):
-        return jnp.sum(jnp.where(eye, row, 0.0), axis=1, keepdims=True)
-
-    def to_row(column):
-        return jnp.sum(jnp.where(eye, column, 0.0), axis=0, keepdims=True)
-
-    expert_id = lax.broadcasted_iota(jnp.int32, (n, tokens), 0)
-    hot = [(expert_id == routes[k : k + 1, :]).astype(f32) for k in range(2)]
-    before = (row_id < col_id).astype(bf)
-    counts = jnp.dot((hot[0] + hot[1]).astype(bf), before, preferred_element_type=f32)
-    slots = [
-        jnp.sum(hot[k] * (counts + (expert_id * cap).astype(f32)), axis=0, keepdims=True)
-        for k in range(2)
-    ]
-    slot_rows = [s.astype(jnp.int32) for s in slots]
-    slot_cols = []
-    for s in slots:
-        near = s.astype(jnp.int32) - me * cap
-        near = jnp.where(near < 0, near + n * cap, near)
-        slot_cols.append(to_column(near.astype(f32)).astype(jnp.int32))
-
-    own = (inner_gate[...].astype(f32) * conv_input[...].astype(f32)).astype(bf).astype(f32)
-    joined[pl.ds(16, tokens), :] = own
-    doc_col = to_column(documents[...].astype(f32))
-    joined_docs[pl.ds(16, tokens), :] = jnp.broadcast_to(doc_col, (tokens, chans))
+    def far(j):
+        src = (routes, route_weights, normed, far_send)[j]
+        dst = (far_routes, far_weights, far_normed, far_sum)[j]
+        return remote(src, dst, far_s.at[j], far_r.at[j], {"sp": twin})
+
+    far(0).start()
+    far(1).start()
+
+    head, body = pl.ds(0, 16), pl.ds(16, tokens - 16)
+
+    def mix(j):
+        if j < 3:
+            part = mixbuf.at[(t, t, partner)[j], body]
+            to = (partner, mate, mate)[j]
+        else:
+            part = mixbuf.at[t, head]
+            to = others[j - 3]
+        return remote(part, part, mix_s.at[j], mix_r.at[j], {"tp": to})
+
+    mix(0).start()
+    mix(1).start()
+
+    @pl.when(me == 0)
+    def _():
+        joined[pl.ds(0, 16), :] = jnp.zeros((16, chans), f32)
+        joined_docs[pl.ds(0, 16), :] = jnp.full((16, chans), -1.0, f32)
 
     @pl.when(me > 0)
     def _():
         for j in range(3):
             halo(j).wait_recv()
-
-    joined[pl.ds(0, 16), :] = (
-        (halo_inner[...].astype(f32) * halo_conv[...].astype(f32)).astype(bf).astype(f32)
-    )
-    halo_col = to_column(halo_docs[...].astype(f32))
-    joined_docs[pl.ds(0, 16), :] = jnp.broadcast_to(halo_col[tokens - 16 :, :], (16, chans))
-    docs_here = joined_docs[pl.ds(16, tokens), :]
-    same_one = (joined_docs[pl.ds(15, tokens), :] == docs_here).astype(f32)
-    same_two = (joined_docs[pl.ds(14, tokens), :] == docs_here).astype(f32)
-    conv_sum = (
-        conv_taps[2:3, :] * own
-        + conv_taps[1:2, :] * joined[pl.ds(15, tokens), :] * same_one
-        + conv_taps[0:1, :] * joined[pl.ds(14, tokens), :] * same_two
-    )
-    mixbuf[t] = (outer_gate[...].astype(f32) * conv_sum).astype(bf)
-
-    def mix(j):
-        return remote(
-            mixbuf.at[t], mixbuf.at[t], mix_s.at[j], mix_r.at[j], {"tp": others[j]}
-        )
-
-    for j in (1, 2, 0):
+        joined[pl.ds(0, 16), :] = (
+            (halo_inner[...].astype(f32) * halo_conv[...].astype(f32)).astype(bf).astype(f32)
+        )
+        halo_col = to_column(halo_docs[...].astype(f32))
+        joined_docs[pl.ds(0, 16), :] = jnp.broadcast_to(halo_col[tokens - 16 :, :], (16, chans))
+
+    convolve(0, 16)
+    for j in (4, 5, 3):
         mix(j).start()
     for load in early:
         load.wait()
-    for j in range(3):
+    mix(0).wait_recv()
+    mix(2).start()
+    for j in range(1, 6):
         mix(j).wait_recv()
     accum = None
     squares = None
@@ -285,22 +332,48 @@
         hidden[...] * lax.rsqrt(feature_total / (4 * lf) + EPS) * ffn_gain[...]
     ).astype(bf)
 
-    def pick_for(e):
+    def pick_for(e, where, rows_of):
         slot_id = lax.broadcasted_iota(jnp.int32, (cap, tokens), 0) + e * cap
-        pick = (slot_id == slot_rows[0]) | (slot_id == slot_rows[1])
+        pick = (slot_id == where[0]) | (slot_id == where[1])
         return jnp.dot(
-            pick.astype(f32).astype(bf), normed[...], preferred_element_type=f32
+            pick.astype(f32).astype(bf), rows_of[...], preferred_element_type=f32
         ).astype(bf)
 
     def dispatch(p):
-        e = (me + p) % n
-        outgoing[e] = pick_for(e)
+        e = me ^ p
+        outgoing[e] = pick_for(e, slot_rows, normed)
         a2a(p).start()
 
-    arrived[t, pl.ds(0, cap), :] = pick_for(me)
+    half = max(1, group // 2)
+    if ISSUE[0] == "Z":
+        far(2).start()
+    arrived[t, pl.ds(0, cap), :] = pick_for(me, slot_rows, normed)
     agy(0).start()
     agm(0).start()
-    each(1, n, dispatch)
+    each(1, half, dispatch)
+    for part in ISSUE.removeprefix("Z"):
+        if part == "Z":
+            far(2).start()
+        else:
+            each(int(part) * half, (int(part) + 1) * half, dispatch)
+    far(0).wait_recv()
+    far(1).wait_recv()
+    far_ranks = ranks(far_routes)
+    far_rows = [v.astype(jnp.int32) for v in places(far_ranks, expert_id)]
+    far_cols = as_columns(places(far_ranks, (expert_id ^ me) + away))
+    far_weight_cols = [to_column(far_weights[k : k + 1, :]) for k in range(2)]
+
+    def forward(p):
+        e = me ^ (p - away)
+        outgoing[e ^ away] = pick_for(e, far_rows, far_normed)
+        a2a(p).start()
+
+    def exchange(g):
+        far(2).wait_recv()
+        arrived[t, span(away), :] = pick_for(me, far_rows, far_normed)
+        agy(away).start()
+        agm(away).start()
+        each(away + 1, n, forward)
 
     def spread(p):
         a2a(p).wait_recv()
@@ -315,27 +388,27 @@
         agm(p).wait_recv()
         agf(p).wait_recv()
 
-    def over_group(i, f):
-        each(i * group, (i + 1) * group, f)
-
     def reduce_mate(i):
         rsm(i, 0).wait_recv()
-        ysend[span_g(i), :] = (mine[0] + mrecv[i, 0].astype(jnp.float32)).astype(jnp.bfloat16)
+        ysend[span_g(i), :] = (mine[i, 0] + mrecv[i, 0].astype(jnp.float32)).astype(jnp.bfloat16)
         over_group(i, lambda p: rsy(p).start())
         rsm(i, 1).wait_recv()
-        mine2[...] = mine[1] + mrecv[i, 1].astype(jnp.float32)
 
     def reduce_partner(i):
         def back(p):
             rsy(p).wait_recv()
             local = pl.ds(pl.multiple_of((p - i * group) * cap, cap), cap)
-            rsend[span(p), :] = (
-                mine2[local, :] + yrecv[span(p), :].astype(jnp.float32)
-            ).astype(jnp.bfloat16)
-
-            @pl.when(p > 0)
+            near = mine[i, 1, local, :] + mrecv[i, 1, local, :].astype(jnp.float32)
+            summed = (near + yrecv[span(p), :].astype(jnp.float32)).astype(jnp.bfloat16)
+
+            @pl.when(p % away > 0)
             def _():
+                rsend[span(p), :] = summed
                 ret(p).start()
+
+            @pl.when(p % away == 0)
+            def _():
+                returned[span(p), :] = summed
 
         over_group(i, back)
 
@@ -355,75 +428,82 @@
                 act[...], wd[:, far], preferred_element_type=jnp.float32
             ).astype(jnp.bfloat16)
             rsm(i, h).start()
-            mine[h] = jnp.dot(act[...], wd[:, near], preferred_element_type=jnp.float32)
-
-    each(1, group, spread)
-    if steps > 1:
-        over_group(1, spread)
-    for load in loads:
-        load.wait()
-
-    def step(i, c):
-        over_group(i, relay)
-
-        @pl.when(i > 0)
-        def _():
-            reduce_mate(i - 1)
-
-        over_group(i, settle)
-
-        @pl.when(i + 2 < steps)
-        def _():
-            over_group(i + 2, spread)
-
-        compute(i)
-
-        @pl.when(i > 0)
-        def _():
-            reduce_partner(i - 1)
-
-        return c
-
-    lax.fori_loop(0, steps, step, 0)
-    reduce_mate(steps - 1)
-
-    weight_cols = [to_column(route_weights[k : k + 1, :]) for k in range(2)]
-
-    def combine(i):
+            mine[i, h] = jnp.dot(act[...], wd[:, near], preferred_element_type=jnp.float32)
+
+    def combine(first, places_of, weights):
         def came(p):
-            @pl.when(p > 0)
+            @pl.when(p % away > 0)
             def _():
                 ret(p).wait_recv()
 
-        over_group(i, came)
-        if i == 0:
-            here = jnp.concatenate(
-                [rsend[0:cap, :], returned[cap:rows, :]], axis=0
-            ) if group > 1 else rsend[0:cap, :]
-        else:
-            here = returned[i * rows : (i + 1) * rows, :]
-        slot_id = lax.broadcasted_iota(jnp.int32, (tokens, rows), 1) + i * rows
-        total = hidden[...]
+        each(first, first + away, came)
+        here = returned[first * cap : (first + away) * cap, :]
+        slot_id = lax.broadcasted_iota(jnp.int32, (tokens, away * cap), 1) + first * cap
+        total = None
         for k in range(2):
-            pick = (slot_id == slot_cols[k]).astype(f32).astype(bf)
-            picked = jnp.dot(pick, here, preferred_element_type=f32)
-            total = total + picked * weight_cols[k]
+            pick = (slot_id == places_of[k]).astype(f32).astype(bf)
+            picked = jnp.dot(pick, here, preferred_element_type=f32) * weights[k]
+            total = picked if total is None else total + picked
         return total
 
-    for i in range(steps - 2):
-        hidden[...] = combine(i)
-    reduce_partner(steps - 1)
-    for i in range(max(0, steps - 2), steps - 1):
-        hidden[...] = combine(i)
-    layer_out[...] = combine(steps - 1).astype(bf)
-
+    def halves(f):
+        def lower(g):
+            each(g * group, g * group + half, f)
+
+        def upper(g):
+            each(g * group + half, (g + 1) * group, f)
+
+        return lower, upper
+
+    def accumulate(g):
+        hidden[...] = hidden[...] + combine(0, slot_cols, weight_cols)
+
+    def send_far(g):
+        far_send[...] = combine(away, far_cols, far_weight_cols).astype(bf)
+        far(3).start()
+
+    def finalize(g):
+        far(3).wait_recv()
+        layer_out[...] = (hidden[...] + far_sum[...].astype(f32)).astype(bf)
+
+    def spread_block(p):
+        @pl.when(p % away > 0)
+        def _():
+            spread(p)
+
+    def load_weights(g):
+        for load in loads:
+            load.wait()
+
+    sa, sb = halves(spread_block)
+    ya, yb = halves(relay)
+    tasks = {
+        "0": lambda g: each(1, group, spread),
+        "S": lambda g: over_group(g, spread_block),
+        "X": exchange,
+        "G": send_far,
+        "a": sa,
+        "b": sb,
+        "Y": lambda g: over_group(g, relay),
+        "y": ya,
+        "z": yb,
+        "T": lambda g: over_group(g, settle),
+        "C": compute,
+        "M": reduce_mate,
+        "P": reduce_partner,
+        "K": accumulate,
+        "F": finalize,
+        "W": load_weights,
+    }
+    for task in PLAN:
+        tasks[task[0]](int(task[1]))
 
     def finish(p):
         agy(p).wait_send()
         agm(p).wait_send()
         agf(p).wait_send()
 
-        @pl.when(p > 0)
+        @pl.when(p % away > 0)
         def _():
             a2a(p).wait_send()
             ret(p).wait_send()
@@ -437,8 +517,11 @@
         rsm(i, 1).wait_send()
 
     each(0, steps, finish_group)
+    for j in range(6):
+        mix(j).wait_send()
+    for j in range(4):
+        far(j).wait_send()
     for j in range(3):
-        mix(j).wait_send()
         tot(j).wait_send()
 
     @pl.when(me < n - 1)
@@ -499,17 +582,26 @@
             pltpu.VMEM((rows, units), bf),
             pltpu.VMEM((steps, 2, rows, lf), bf),
             pltpu.VMEM((steps, 2, rows, lf), bf),
-            pltpu.VMEM((2, rows, lf), f32),
+            pltpu.VMEM((steps, 2, rows, lf), f32),
             pltpu.VMEM((n * cap, lf), bf),
             pltpu.VMEM((n * cap, lf), bf),
-            pltpu.VMEM((rows, lf), f32),
             pltpu.VMEM((n * cap, lf), bf),
             dma((5,)),
         ]
         + [dma((n,))] * 8
         + [dma((steps, 2))] * 2
         + [dma((n,))] * 4
-        + [dma((3,))] * 6,
+        + [dma((3,))] * 2
+        + [dma((6,))] * 2
+        + [dma((3,))] * 2
+        + [dma((4,))] * 2
+        + [
+            pltpu.VMEM((2, tokens), jnp.int32),
+            pltpu.VMEM((2, tokens), f32),
+            pltpu.VMEM((tokens, lf), bf),
+            pltpu.VMEM((tokens, lf), bf),
+            pltpu.VMEM((tokens, lf), bf),
+        ],
         compiler_params=pltpu.CompilerParams(
             collective_id=0, has_side_effects=True, vmem_limit_bytes=58 * 1024 * 1024
         ),

time: 93.5 us -> 83.6 us (0.89)
  Pallas kernels: 91.6 us -> 81.3 us
    pallas_call x1, Pallas kernels: 91.6 us -> 81.3 us  [per_device(): pl.pallas_call(functools.partial(layer_kernel, n, group), out_shape=jax.S...]
where the time goes in v1:
time: 83.6 us; the launch traced here: 82.9 us
  Pallas kernels  81.3 us (97%)
  local copies, waits for them, and re-layouts  1.67 us (2%)
    pallas_call x1, Pallas kernels, per_device(): pl.pallas_call(functools.partial(layer_kernel, n, group), out_shape=jax.S...  81.3 us

profile of v1, /device:TPU:0, one launch (start us, length us, event | category | flops | bytes accessed | tf_op | source)
XLA Modules:
  0.0 82.9 jit_solution(1085607091275288705)
XLA Ops:
  0.0 81.3 %layer.1 = bf16[256,512]{1,0:T(8,128)(2,1)} custom-call(bf16[256,512]{1,0:T(8,128)(2,1)} %residual_hbm.1, bf16[256,128]{1,0:T(8,128)(2,1)} %conv_input.1, bf16[256,128]{1,0:T(8,128)(2,1)} %outer_gate.1, bf16[256,128]{1,0:T(8,128)(2,1)} %inner_gate.1, s32[1,256]{1,0:T(1,128)} %bitcast.9, f32[3,128]{1,0:T(4,128)} %conv_taps.1, f32[1,512]{1,0:T(1,128)} %bitcast.5, ...), custom_call_target="tpu_custom_call" | custom-call | tf_op jit(solution)/shard_map/layer/pallas_call | solution.py:559
  81.3 1.7 %copy.16 = bf16[256,512]{1,0:T(8,128)(2,1)} copy(bf16[256,512]{1,0:T(8,128)(2,1)} %layer.1) | data formatting | bytes 524288

commit v2 on v1

--- a/solution.py
+++ b/solution.py
@@ -23,16 +23,16 @@
     n,
     group,
     residual_hbm,
-    conv_input,
-    outer_gate,
-    inner_gate,
-    documents,
-    conv_taps,
-    mixer_gain,
+    conv_input_hbm,
+    outer_gate_hbm,
+    inner_gate_hbm,
+    documents_hbm,
+    conv_taps_hbm,
+    mixer_gain_hbm,
     ow_hbm,
-    ffn_gain,
-    routes,
-    route_weights,
+    ffn_gain_hbm,
+    routes_hbm,
+    route_weights_hbm,
     gate_hbm,
     up_hbm,
     down_hbm,
@@ -45,7 +45,7 @@
     joined,
     joined_docs,
     mixbuf,
-    totals,
+    gains,
     hidden,
     normed,
     outgoing,
@@ -89,6 +89,16 @@
     far_normed,
     far_send,
     far_sum,
+    conv_input,
+    outer_gate,
+    inner_gate,
+    documents,
+    conv_taps,
+    mixer_gain,
+    ffn_gain,
+    routes,
+    route_weights,
+    in_sem,
 ):
     me = lax.axis_index("sp")
     t = lax.axis_index("tp")
@@ -104,6 +114,16 @@
     rows = group * cap
     steps = n // group
 
+    barrier = pltpu.get_barrier_semaphore()
+
+    def greet(q, c):
+        pl.semaphore_signal(barrier, inc=1, device_id={"sp": me ^ q}, device_id_type=MESH)
+        return c
+
+    lax.fori_loop(1, n, greet, 0)
+    for other in (mate, partner, across):
+        pl.semaphore_signal(barrier, inc=1, device_id={"tp": other}, device_id_type=MESH)
+
     early = [
         pltpu.make_async_copy(ow_hbm, ow, w_sem.at[3]),
         pltpu.make_async_copy(residual_hbm, residual, w_sem.at[4]),
@@ -113,18 +133,26 @@
         pltpu.make_async_copy(up_hbm.at[0], wu, w_sem.at[1]),
         pltpu.make_async_copy(down_hbm.at[0], wd, w_sem.at[2]),
     ]
-    for load in early + loads:
+    staged = [
+        pltpu.make_async_copy(src, dst, in_sem.at[j])
+        for j, (src, dst) in enumerate(
+            (
+                (conv_input_hbm, conv_input),
+                (inner_gate_hbm, inner_gate),
+                (outer_gate_hbm, outer_gate),
+                (documents_hbm, documents),
+                (conv_taps_hbm, conv_taps),
+                (routes_hbm, routes),
+                (route_weights_hbm, route_weights),
+                (mixer_gain_hbm, mixer_gain),
+                (ffn_gain_hbm, ffn_gain),
+            )
+        )
+    ]
+    for load in staged + early + loads:
         load.start()
-
-    barrier = pltpu.get_barrier_semaphore()
-
-    def greet(q, c):
-        pl.semaphore_signal(barrier, inc=1, device_id={"sp": me ^ q}, device_id_type=MESH)
-        return c
-
-    lax.fori_loop(1, n, greet, 0)
-    for other in (mate, partner, across):
-        pl.semaphore_signal(barrier, inc=1, device_id={"tp": other}, device_id_type=MESH)
+    for load in staged:
+        load.wait()
 
     def remote(src, dst, s, r, dev):
         return pltpu.make_async_remote_copy(
@@ -277,6 +305,15 @@
 
     mix(0).start()
     mix(1).start()
+
+    def tot(j):
+        return remote(
+            ffn_gain, gains.at[t], tot_s.at[j], tot_r.at[j], {"tp": others[j]}
+        )
+
+    for j in range(3):
+        tot(j).start()
+    gains[t] = ffn_gain[...]
 
     @pl.when(me == 0)
     def _():
@@ -314,23 +351,7 @@
         squares = square if squares is None else squares + square
     mix_scale = lax.rsqrt(squares / (4 * chans) + EPS)
     hidden[...] = residual[...].astype(f32) + accum * mix_scale
-    state = hidden[...]
-    total = to_row(jnp.sum(state * state, axis=1, keepdims=True))
-    totals[t] = jnp.broadcast_to(total, (8, tokens))
-
-    def tot(j):
-        return remote(
-            totals.at[t], totals.at[t], tot_s.at[j], tot_r.at[j], {"tp": others[j]}
-        )
-
-    for j in (1, 2, 0):
-        tot(j).start()
-    for j in range(3):
-        tot(j).wait_recv()
-    feature_total = to_column((totals[0] + totals[1] + totals[2] + totals[3])[0:1, :])
-    normed[...] = (
-        hidden[...] * lax.rsqrt(feature_total / (4 * lf) + EPS) * ffn_gain[...]
-    ).astype(bf)
+    normed[...] = (hidden[...] * ffn_gain[...]).astype(bf)
 
     def pick_for(e, where, rows_of):
         slot_id = lax.broadcasted_iota(jnp.int32, (cap, tokens), 0) + e * cap
@@ -414,12 +435,20 @@
 
     def compute(i):
         whole = jnp.concatenate([arrived[q, span_g(i), :] for q in range(4)], axis=1)
+        squares = None
+        for q in range(4):
+            piece = arrived[q, span_g(i), :].astype(f32) * gains[q]
+            square = jnp.sum(piece * piece, axis=1, keepdims=True)
+            squares = square if squares is None else squares + square
+        scale = lax.rsqrt(squares / (4 * lf) + EPS)
         for j in range(units // 128):
             cols = slice(j * 128, (j + 1) * 128)
             w = jnp.concatenate([wg[:, cols], wu[:, cols]], axis=1)
             both = jnp.dot(whole, w, preferred_element_type=jnp.float32)
             g = both[:, :128]
-            act[:, cols] = (g * jax.nn.sigmoid(g) * both[:, 128:]).astype(jnp.bfloat16)
+            g = g * scale
+            up = both[:, 128:] * scale
+            act[:, cols] = (g * jax.nn.sigmoid(g) * up).astype(jnp.bfloat16)
         for h in range(2):
             qa = (1 - a) if h == 0 else a
             far = pl.ds(pl.multiple_of((2 * qa + 1 - b) * lf, lf), lf)
@@ -472,6 +501,10 @@
             spread(p)
 
     def load_weights(g):
+        for j in range(3):
+            tot(j).wait_recv()
+        for q in range(4):
+            gains[q] = 1.0 / gains[q]
         for load in loads:
             load.wait()
 
@@ -558,8 +591,8 @@
     vmem, hbm = pl.BlockSpec(memory_space=pltpu.VMEM), pl.BlockSpec(memory_space=pl.ANY)
     return pl.pallas_call(
         functools.partial(layer_kernel, n, group),
-        out_shape=jax.ShapeDtypeStruct((tokens, lf), bf),
-        in_specs=[hbm] + [vmem] * 6 + [hbm] + [vmem] * 3 + [hbm] * 3,
+        out_shape=pltpu.VMEM((tokens, lf), bf),
+        in_specs=[hbm] * 14,
         out_specs=vmem,
         scratch_shapes=[
             pltpu.VMEM((tokens, lf), bf),
@@ -570,7 +603,7 @@
             pltpu.VMEM((tokens + 16, chans), f32),
             pltpu.VMEM((tokens + 16, chans), f32),
             pltpu.VMEM((4, tokens, chans), bf),
-            pltpu.VMEM((4, 8, tokens), f32),
+            pltpu.VMEM((4, 1, lf), f32),
             pltpu.VMEM((tokens, lf), f32),
             pltpu.VMEM((tokens, lf), bf),
             pltpu.VMEM((n, cap, lf), bf),
@@ -601,6 +634,16 @@
             pltpu.VMEM((tokens, lf), bf),
             pltpu.VMEM((tokens, lf), bf),
             pltpu.VMEM((tokens, lf), bf),
+            pltpu.VMEM((tokens, chans), bf),
+            pltpu.VMEM((tokens, chans), bf),
+            pltpu.VMEM((tokens, chans), bf),
+            pltpu.VMEM((1, tokens), jnp.int32),
+            pltpu.VMEM((3, chans), f32),
+            pltpu.VMEM((1, 4 * chans), f32),
+            pltpu.VMEM((1, lf), f32),
+            pltpu.VMEM((2, tokens), jnp.int32),
+            pltpu.VMEM((2, tokens), f32),
+            dma((9,)),
         ],
         compiler_params=pltpu.CompilerParams(
             collective_id=0, has_side_effects=True, vmem_limit_bytes=58 * 1024 * 1024

time: 83.6 us -> 79.4 us (0.950)
  Pallas kernels: 81.3 us -> 78.6 us
  local copies, waits for them, and re-layouts: 1.67 us -> 0.71 us
    pallas_call x1, Pallas kernels: 81.3 us -> 78.6 us  [per_device(): pl.pallas_call(functools.partial(layer_kernel, n, group), out_shape=pltpu...]
    unnamed x1, local copies, waits for them, and re-layouts: 1.67 us -> 0.71 us
where the time goes in v2:
time: 79.4 us; the launch traced here: 79.3 us
  Pallas kernels  78.6 us (99%)
    pallas_call x1, Pallas kernels, per_device(): pl.pallas_call(functools.partial(layer_kernel, n, group), out_shape=pltpu...  78.6 us

profile of v2, /device:TPU:0, one launch (start us, length us, event | category | flops | bytes accessed | tf_op | source)
XLA Modules:
  0.0 79.3 jit_solution(18155160827937726633)
XLA Ops:
  0.0 78.6 %layer.1 = bf16[256,512]{1,0:T(8,128)(2,1)S(1)} custom-call(bf16[256,512]{1,0:T(8,128)(2,1)} %residual_hbm.1, bf16[256,128]{1,0:T(8,128)(2,1)} %conv_input_hbm.1, bf16[256,128]{1,0:T(8,128)(2,1)} %outer_gate_hbm.1, bf16[256,128]{1,0:T(8,128)(2,1)} %inner_gate_hbm.1, s32[1,256]{1,0:T(1,128)} %bitcast.9, f32[3,128]{1,0:T(4,128)} %conv_taps_hbm.1, ...), custom_call_target="tpu_custom_call" | custom-call | tf_op jit(solution)/shard_map/layer/pallas_call | solution.py:592
  78.6 0.7 copy.16

commit v3 on v2

--- a/solution.py
+++ b/solution.py
@@ -13,8 +13,8 @@
 
 ISSUE = "Z123"
 PLAN = (
-    "00", "S1", "W0", "X0", "Y0", "T0", "C0", "S2", "S3", "Y1", "T1", "C1",
-    "Y2", "T2", "C2", "M2", "Y3", "T3", "C3", "M3", "M1", "M0", "P2", "P3",
+    "00", "W0", "Y0", "S1", "X0", "T0", "C0", "S2", "S3", "Y1", "T1", "C1",
+    "Y2", "T2", "C2", "Y3", "M2", "T3", "C3", "M3", "M1", "M0", "P2", "P3",
     "G0", "P1", "P0", "K0", "F0",
 )
 

time: 79.4 us -> 78.9 us (level)
  no operation moved by 1% of the time
where the time goes in v3:
time: 78.9 us; the launch traced here: 78.7 us
  Pallas kernels  78 us (99%)
    pallas_call x1, Pallas kernels, per_device(): pl.pallas_call(functools.partial(layer_kernel, n, group), out_shape=pltpu...  78 us

profile of v3, /device:TPU:0, one launch (start us, length us, event | category | flops | bytes accessed | tf_op | source)
XLA Modules:
  0.0 78.7 jit_solution(15164577497580453851)
XLA Ops:
  0.0 78.0 %layer.1 = bf16[256,512]{1,0:T(8,128)(2,1)S(1)} custom-call(bf16[256,512]{1,0:T(8,128)(2,1)} %residual_hbm.1, bf16[256,128]{1,0:T(8,128)(2,1)} %conv_input_hbm.1, bf16[256,128]{1,0:T(8,128)(2,1)} %outer_gate_hbm.1, bf16[256,128]{1,0:T(8,128)(2,1)} %inner_gate_hbm.1, s32[1,256]{1,0:T(1,128)} %bitcast.9, f32[3,128]{1,0:T(4,128)} %conv_taps_hbm.1, ...), custom_call_target="tpu_custom_call" | custom-call | tf_op jit(solution)/shard_map/layer/pallas_call | solution.py:592
  78.0 0.7 copy.16
